TPU v7x, 32 devices: a whole 2x2x4 slice. The times are simulated.
32 devices in a mesh: sp: 8 (over z, core), tp: 4 (over y, x).
Axes of the slice: x: 2, y: 2, z: 4, core: 2. Of those that a mesh axis runs over, the one named last changes fastest.
Arguments:
- queries: bfloat16 [4096, 1024], P('sp', 'tp'), may hold values from -20 to 20
- key_vectors: bfloat16 [4096, 1024], P('sp', 'tp'), may hold values from -20 to 20
- value_vectors: bfloat16 [4096, 1024], P('sp', 'tp'), may hold values from -6 to 6
- log_gate_sums: float32 [4096, 16], P('sp', 'tp'), may hold values from -588 to 0, as said below
- residual: bfloat16 [4096, 2048], P('sp', 'tp'), may hold values from -24 to 24
- out_weight: bfloat16 [1024, 2048], P(None, 'tp'), may hold values from -0.75 to 0.75
- norm_gain: bfloat16 [2048], replicated, may hold values from 0.099609375 to 1.8984375
- routes: int32 [4096, 2], P('sp'), may hold values from 0 to 31, all different within a row; in each aligned block of 512 rows (0 to 511, 512 to 1023, ...) at most 40 rows name the same one
- route_weight: float32 [4096, 2], P('sp'), may hold values from 0.5 to 1.5
- expert_gate: bfloat16 [32, 2048, 512], P('sp', None, 'tp'), may hold values from -0.125 to 0.125
- expert_up: bfloat16 [32, 2048, 512], P('sp', None, 'tp'), may hold values from -0.125 to 0.125
- expert_down: bfloat16 [32, 512, 2048], P('sp', None, 'tp'), may hold values from -0.25 to 0.25
- shared_gate: bfloat16 [2048, 512], P(None, 'tp'), may hold values from -0.125 to 0.125
- shared_up: bfloat16 [2048, 512], P(None, 'tp'), may hold values from -0.125 to 0.125
- shared_down: bfloat16 [512, 2048], P(None, 'tp'), may hold values from -0.25 to 0.25
Outputs:
- layer_out: bfloat16 [4096, 2048], P('sp', 'tp')
Inputs may be any that keep to these rules, and one draw needn't show every extreme that they name: `log_gate_sums`: for each head the values do not rise along the positions. `routes`: each row names 2 different experts; among the rows of one index of sp no expert is named by more than 40 rows, a bound that some block reaches.
All inputs are finite; a program needn't handle non-finite values.
Results may differ from a plain program's by a relative error of at most 0.014.
Values may be sent and summed in bfloat16 or wider, within the bound.
A program may use at most 64 MiB of HBM per device.

v0:
```python
import math
import jax
import jax.numpy as jnp
from jax import lax
from jax.sharding import PartitionSpec as P

HDIM = 64
EPSILON = 1e-06


def silu_gate(gate_part, up_part):
    return jax.nn.silu(gate_part) * up_part


def slot_targets(routes, experts_all, capacity):
    flat_routes = routes.reshape(-1)
    onehot = (flat_routes[:, None] == jnp.arange(experts_all, dtype=jnp.int32)[None, :]).astype(
        jnp.int32
    )
    before = jnp.cumsum(onehot, axis=0) - onehot
    return flat_routes * capacity + jnp.sum(before * onehot, axis=1)


def keep_state(fold_state):
    return fold_state


def shards(
    queries,
    key_vectors,
    value_vectors,
    log_gate_sums,
    residual,
    out_weight,
    norm_gain,
    routes,
    route_weight,
    expert_gate,
    expert_up,
    expert_down,
    shared_gate,
    shared_up,
    shared_down,
):
    tok_dev = queries.shape[0]
    head_dim = HDIM
    local_heads = log_gate_sums.shape[1]
    local_width = residual.shape[1]
    model_width = norm_gain.shape[0]
    score_scale = head_dim ** (-0.5)
    seq_first = lax.axis_index("sp") * tok_dev
    query_heads = queries.reshape(tok_dev, local_heads, head_dim)
    query_pos = seq_first + jnp.arange(tok_dev, dtype=jnp.int32)
    own_gates = log_gate_sums.T
    all_gates = lax.all_gather(log_gate_sums, "sp", axis=0, tiled=True)
    initial = (
        jnp.full((local_heads, tok_dev), -1e30, jnp.float32),
        jnp.zeros((local_heads, tok_dev), jnp.float32),
        jnp.zeros((local_heads, tok_dev, head_dim), jnp.float32),
    )
    key_heads = key_vectors.reshape(tok_dev, local_heads, head_dim)
    value_heads = value_vectors.reshape(tok_dev, local_heads, head_dim)
    key_part = lax.all_gather(key_heads, "sp", axis=0, tiled=True)
    value_part = lax.all_gather(value_heads, "sp", axis=0, tiled=True)
    part_rows = key_part.shape[0]
    block_size = math.gcd(part_rows, 512)
    key_blocks = key_part.reshape(part_rows // block_size, block_size, local_heads, head_dim)
    value_blocks = value_part.reshape(part_rows // block_size, block_size, local_heads, head_dim)

    def one_block(fold_state, inputs):
        key_block, value_block, block_number = inputs
        block_first = block_number * block_size

        def compute(old_state):
            running_max, weight_total, summed = old_state
            gate_block = lax.dynamic_slice_in_dim(all_gates, block_first, block_size, 0).T
            scores = (
                jnp.einsum(
                    "qhd,khd->hqk", query_heads, key_block, preferred_element_type=jnp.float32
                )
                * score_scale
            )
            scores = scores + own_gates[:, :, None] - gate_block[:, None, :]
            key_pos = block_first + jnp.arange(block_size, dtype=jnp.int32)
            allowed = (key_pos[None, :] <= query_pos[:, None])[None]
            newmax = jnp.maximum(running_max, jnp.max(jnp.where(allowed, scores, -jnp.inf), axis=2))
            factor = jnp.exp(running_max - newmax)
            weight = jnp.where(allowed, jnp.exp(scores - newmax[:, :, None]), 0.0)
            weight_total = weight_total * factor + jnp.sum(weight, axis=2)
            summed = summed * factor[:, :, None] + jnp.einsum(
                "hqk,khd->hqd",
                weight.astype(jnp.bfloat16),
                value_block,
                preferred_element_type=jnp.float32,
            )
            return (newmax, weight_total, summed)

        useful = block_first <= seq_first + tok_dev - 1
        return (lax.cond(useful, compute, keep_state, fold_state), None)

    numbers = jnp.arange(part_rows // block_size, dtype=jnp.int32)
    result_state, _ = lax.scan(one_block, initial, (key_blocks, value_blocks, numbers))
    running_max, weight_total, summed = result_state
    attended = (summed / weight_total[:, :, None]).astype(jnp.bfloat16)
    attended = attended.transpose(1, 0, 2).reshape(tok_dev, local_heads * head_dim)
    weight_rows = out_weight
    projected = jnp.dot(
        lax.all_gather(attended, "tp", axis=1, tiled=True),
        weight_rows,
        preferred_element_type=jnp.float32,
    )
    mid = (residual.astype(jnp.float32) + projected).astype(jnp.bfloat16)
    mid_wide = mid.astype(jnp.float32)
    feature_first = lax.axis_index("tp") * local_width
    squares = lax.psum(jnp.sum(mid_wide * mid_wide, axis=1), "tp")
    inverse = lax.rsqrt(squares / model_width + EPSILON)
    own_gain = lax.dynamic_slice_in_dim(norm_gain, feature_first, local_width, 0).astype(
        jnp.float32
    )
    normed_own = (mid_wide * inverse[:, None] * own_gain[None, :]).astype(jnp.bfloat16)
    normed = lax.all_gather(normed_own, "tp", axis=1, tiled=True)
    shared_mid = silu_gate(
        jnp.dot(normed, shared_gate, preferred_element_type=jnp.float32),
        jnp.dot(normed, shared_up, preferred_element_type=jnp.float32),
    ).astype(jnp.bfloat16)
    weight_rows = shared_down
    shared_out = jnp.dot(
        lax.all_gather(shared_mid, "tp", axis=1, tiled=True),
        weight_rows,
        preferred_element_type=jnp.float32,
    )
    exp_dev = expert_gate.shape[0]
    sp_count = lax.axis_size("sp")
    experts_all = exp_dev * sp_count
    top_count = routes.shape[1]
    capacity = 5 * tok_dev * top_count // (4 * experts_all)
    targets = slot_targets(routes, experts_all, capacity)
    owners = (
        jnp.full((experts_all * capacity,), tok_dev, jnp.int32)
        .at[targets]
        .set(jnp.arange(tok_dev * top_count, dtype=jnp.int32) // top_count)
    )
    padded = jnp.concatenate(
        [normed_own, jnp.zeros((1, normed_own.shape[1]), jnp.bfloat16)], axis=0
    )
    outgoing = padded[owners].reshape(sp_count, exp_dev, capacity, normed_own.shape[1])
    rows_all = lax.all_gather(
        lax.all_to_all(outgoing, "sp", split_axis=0, concat_axis=0, tiled=True),
        "tp",
        axis=3,
        tiled=True,
    )
    gate_part = jnp.einsum(
        "secd,edf->secf", rows_all, expert_gate, preferred_element_type=jnp.float32
    )
    up_part = jnp.einsum("secd,edf->secf", rows_all, expert_up, preferred_element_type=jnp.float32)
    hidden = silu_gate(gate_part, up_part).astype(jnp.bfloat16)
    hidden_all = lax.all_gather(hidden, "tp", axis=3, tiled=True)
    produced = jnp.einsum(
        "secf,efd->secd", hidden_all, expert_down, preferred_element_type=jnp.float32
    ).astype(jnp.bfloat16)
    returned = lax.all_to_all(produced, "sp", split_axis=0, concat_axis=0, tiled=True)
    returned_flat = returned.reshape(experts_all * capacity, local_width)
    picked = returned_flat[targets].astype(jnp.float32).reshape(tok_dev, top_count, local_width)
    routed = jnp.sum(picked * route_weight[:, :, None], axis=1)
    return (mid_wide + shared_out + routed).astype(jnp.bfloat16)


def solution(mesh):
    placed = (
        P("sp", "tp"),
        P("sp", "tp"),
        P("sp", "tp"),
        P("sp", "tp"),
        P("sp", "tp"),
        P(None, "tp"),
        P(),
        P("sp", None),
        P("sp", None),
        P("sp", None, "tp"),
        P("sp", None, "tp"),
        P("sp", None, "tp"),
        P(None, "tp"),
        P(None, "tp"),
        P(None, "tp"),
    )
    return jax.shard_map(
        shards, mesh=mesh, in_specs=placed, out_specs=P("sp", "tp"), check_vma=False
    )
```

profile of v0, /device:TPU:0, one launch (start us, length us, event | category | flops | bytes accessed | tf_op | source)
XLA Modules:
  0.0 383.8 jit_solution(4985606902853403032)
XLA Ops:
  11.8 15.9 %all_gather.25 = f32[4096,4]{0,1:T(4,128)S(1)} all-gather(f32[512,4]{0,1:T(4,128)S(1)} %copy-done.9), channel_id=1, replica_groups=mesh['sp'=8,'tp'=4] {'sp'}, dimensions={0}, use_global_device_ids=true | all-gather | bytes 73728 | tf_op jit(solution)/shard_map/all_gather | solution.py:55
  27.7 13.3 %all-gather.9.cloned.1.call-done = bf16[4096,4,64]{0,2,1:T(8,128)(2,1)} async-done(((bf16[512,4,64]{0,2,1:T(8,128)(2,1)}), bf16[4096,4,64]{0,2,1:T(8,128)(2,1)}) %all-gather.9.cloned.1.call-update) | async-done | bytes 2097168 | tf_op jit(solution)/shard_map/all_gather | solution.py:64
  41.0 3.2 copy.57
  44.2 27.0 %all-gather.7.cloned.1.call-done = bf16[4096,4,64]{0,2,1:T(8,128)(2,1)} async-done(((bf16[512,4,64]{0,2,1:T(8,128)(2,1)}), bf16[4096,4,64]{0,2,1:T(8,128)(2,1)}) %all-gather.7.cloned.1.call-update) | async-done | bytes 2097168 | tf_op jit(solution)/shard_map/all_gather | solution.py:63
  71.3 3.2 copy.58
  74.6 16.6 %while.17 = (s32[]{:T(128)}, f32[4,512]{1,0:T(4,128)S(1)}, f32[4,512]{1,0:T(4,128)S(1)}, f32[4,512,64]{1,2,0:T(8,128)S(1)}, s32[8]{0:T(128)S(1)}, /*index=5*/s32...) while((s32[]{:T(128)}, f32[4,512]{1,0:T(4,128)S(1)}, ...), condition=%wide.region_5.6_spmd.clone, body=%wide.region_0.5_spmd.clone.sunk | while | flops 286790656 | bytes 15676785 | solution.py:102
  75.8 6.3 %conditional.3 = ((f32[4,512]{1,0:T(4,128)S(1)}, f32[4,512]{1,0:T(4,128)S(1)}, f32[4,512,64]{1,2,0:T(8,128)S(1)})) conditional(s32[]{:T(128)} %convert_element_type.105, (f32[4,512]{1,0:T(4,128)S(1)}, f32[4,512]{1,0:T(4,128)S(1)}, f32[4,512,64]{1,2,0:T(8,128)S(1)}) %tuple.50, (s32[]{:T(128)}, s32[]{:T(128)}, bf16[8,512,4,64]{1,3,2,0:T(8,128)(2,1)}, ...), branch_computations={%region_1.1_spmd, %region_2.4_spmd} | conditional | flops 286790656 | bytes 15674446 | solution.py:99
  92.0 9.0 %reduce-window.6 = s32[32,8,128]{2,1,0:T(8,128)S(1)} reduce-window(s32[32,8,128]{2,1,0:T(8,128)S(1)} %fusion.56, s32[]{:T(128)} %constant.93.clone.1), window={size=1x1x128 pad=0_0x0_0x127_0}, to_apply=%region_8.9 | reduce-window | flops 4161536 | bytes 262148 | tf_op jit(solution)/shard_map/reduce-window
  101.9 4.3 %scatter_custom_fusion = s32[1280]{0:T(1024)S(1)} fusion(s32[1024]{0:T(1024)S(1)} %bitcast.129, s32[1024]{0:T(1024)S(1)} %add_select_fusion, s32[]{:T(128)} %constant.98.clone.1), kind=kCustom, calls=%fused_computation.75 | custom fusion | bytes 5124 | tf_op jit(solution)/shard_map/scatter | solution.py:141
  107.0 54.9 %all-gather.11.cloned.1.call-done = bf16[512,1024]{0,1:T(8,128)(2,1)} async-done(((bf16[512,256]{0,1:T(8,128)(2,1)}), bf16[512,1024]{0,1:T(8,128)(2,1)}) %all-gather.11.cloned.1.call-update) | async-done | bytes 1048592 | tf_op jit(solution)/shard_map/all_gather | solution.py:108
  161.9 2.5 fusion.50
  164.4 8.9 %psum.7 = f32[512]{0:T(512)S(1)} all-reduce(f32[512]{0:T(512)S(1)} %get-tuple-element.335), channel_id=1, replica_groups=mesh['sp'=8,'tp'=4] {'tp'}, use_global_device_ids=true, to_apply=%region_7.8 | all-reduce | flops 512 | bytes 4096 | tf_op jit(solution)/shard_map/psum | solution.py:115
  173.6 4.7 %gather_fusion = bf16[1280,512]{1,0:T(8,128)(2,1)} fusion(bf16[513,512]{1,0:T(8,128)(2,1)S(1)} %concatenate.3, s32[2048]{0:T(1024)S(1)} %pad_clamp_fusion), kind=kCustom, calls=%fused_computation | custom fusion | bytes 2626560 | tf_op jit(solution)/shard_map/gather | solution.py:146
  178.4 36.8 %all_to_all.10 = bf16[8,4,40,512]{3,2,1,0:T(8,128)(2,1)S(1)} all-to-all(bf16[8,4,40,512]{3,2,1,0:T(8,128)(2,1)} %bitcast.116), channel_id=1, replica_groups=mesh['sp'=8,'tp'=4] {'sp'}, dimensions={0} | all-to-all | bytes 2621440 | tf_op jit(solution)/shard_map/all_to_all | solution.py:148
  216.6 59.0 %all-gather.15.cloned.1.call-done = bf16[8,4,40,2048]{3,2,0,1:T(8,128)(2,1)} async-done(((bf16[8,4,40,512]{3,2,0,1:T(8,128)(2,1)}), bf16[8,4,40,2048]{3,2,0,1:T(8,128)(2,1)}) %all-gather.15.cloned.1.call-update) | async-done | bytes 5242896 | tf_op jit(solution)/shard_map/all_gather | solution.py:147
  275.7 4.8 %fusion.37 = f32[8,4,40,128]{3,2,0,1:T(8,128)S(1)} fusion(bf16[8,4,40,2048]{3,2,0,1:T(8,128)(2,1)} %all-gather.15.cloned.1.call-done, bf16[4,2048,128]{2,1,0:T(8,128)(2,1)} %param.28), kind=kOutput, calls=%fused_computation.48 | convolution fusion | flops 671088640 | bytes 7995392 | tf_op jit(solution)/shard_map/secd,edf->secf/dot_general | solution.py:153
  283.9 28.1 %all-gather.17.cloned.1.call-done = bf16[8,4,40,512]{3,2,0,1:T(8,128)(2,1)} async-done(((bf16[8,4,40,128]{3,2,0,1:T(8,128)(2,1)}), bf16[8,4,40,512]{3,2,0,1:T(8,128)(2,1)}) %all-gather.17.cloned.1.call-update) | async-done | bytes 1310736 | tf_op jit(solution)/shard_map/all_gather | solution.py:158
  315.3 4.6 %all-to-all-start.1 = ((bf16[8,4,40,512]{3,2,1,0:T(8,128)(2,1)}), bf16[8,4,40,512]{3,2,1,0:T(8,128)(2,1)S(1)}, u32[]{:S(2)}, u32[]{:S(2)}) async-start(bf16[8,4,40,512]{3,2,1,0:T(8,128)(2,1)} %copy.45), calls=%async_computation.1 | async-start | bytes 2621440 | tf_op jit(solution)/shard_map/all_to_all | solution.py:162
  320.8 27.9 %all-gather.13.cloned.1.call-done = bf16[512,2048]{1,0:T(8,128)(2,1)} async-done(((bf16[512,512]{1,0:T(8,128)(2,1)}), bf16[512,2048]{1,0:T(8,128)(2,1)}) %all-gather.13.cloned.1.call-update) | async-done | bytes 2097168 | tf_op jit(solution)/shard_map/all_gather | solution.py:121
  348.7 2.5 fusion.62
  352.0 10.6 %all_gather.29 = bf16[512,512]{1,0:T(8,128)(2,1)} all-gather(bf16[512,128]{1,0:T(8,128)(2,1)S(1)} %fusion.49), channel_id=1, replica_groups=mesh['sp'=8,'tp'=4] {'tp'}, dimensions={1}, use_global_device_ids=true | all-gather | bytes 655360 | tf_op jit(solution)/shard_map/all_gather | solution.py:128
  362.6 5.1 %gather_fusion.1 = bf16[1024,512]{1,0:T(8,128)(2,1)} fusion(bf16[1280,512]{1,0:T(8,128)(2,1)S(1)} %bitcast.115, s32[1024]{0:T(1024)S(1)} %broadcast_clamp_fusion), kind=kCustom, calls=%fused_computation.1 | custom fusion | bytes 2101248 | tf_op jit(solution)/shard_map/gather | solution.py:164
  367.7 3.4 reshape.124
  371.1 4.5 %multiply_reduce_fusion = f32[512,512]{1,0:T(8,128)S(1)} fusion(f32[512,2,512]{2,1,0:T(2,128)} %reshape.124, f32[512,2]{1,0:T(8,128)S(1)} %copy-done.7), kind=kLoop, calls=%fused_computation.38 | loop fusion | flops 786432 | bytes 3149824 | tf_op jit(solution)/shard_map/reduce_sum | solution.py:165
  (113 shorter events, 29.9 us)
Async XLA Ops:
  6.5 305.4 %copy-start = (bf16[4,512,512]{2,1,0:T(8,128)(2,1)S(1)}, bf16[4,512,512]{2,1,0:T(8,128)(2,1)}, u32[]{:S(2)}) copy-start(bf16[4,512,512]{2,1,0:T(8,128)(2,1)} %param.30) | copy-start | bytes 6291460
  6.5 5.1 %copy-start.10 = (bf16[512,256]{1,0:T(8,128)(2,1)S(1)}, bf16[512,256]{1,0:T(8,128)(2,1)}, u32[]{:S(2)}) copy-start(bf16[512,256]{1,0:T(8,128)(2,1)} %param.19) | copy-start | bytes 786436
  6.5 5.2 %copy-start.9 = (f32[512,4]{0,1:T(4,128)S(1)}, f32[512,4]{0,1:T(4,128)}, u32[]{:S(2)}) copy-start(f32[512,4]{0,1:T(4,128)} %param.22) | copy-start | bytes 24580
  6.5 34.5 %all-gather.9.cloned.1.call-start = ((), (), s32[]{:S(2)}) async-start(), calls=%async_computation.3 | async-start | bytes 2359296 | tf_op jit(solution)/shard_map/all_gather | solution.py:64
  8.5 62.8 %all-gather.7.cloned.1.call-start = ((), (), s32[]{:S(2)}) async-start(), calls=%async_computation.2 | async-start | bytes 2359296 | tf_op jit(solution)/shard_map/all_gather | solution.py:63
  10.4 151.5 %all-gather.11.cloned.1.call-start = ((), (), s32[]{:S(2)}) async-start(), calls=%async_computation.4 | async-start | bytes 1310720 | tf_op jit(solution)/shard_map/all_gather | solution.py:108
  74.6 26.8 %copy-start.11 = (s32[512,2]{0,1:T(2,128)S(1)}, s32[512,2]{0,1:T(2,128)}, u32[]{:S(2)}) copy-start(s32[512,2]{0,1:T(2,128)} %param.26) | copy-start | bytes 12292
  92.0 183.7 %all-gather.15.cloned.1.call-start = ((), (), s32[]{:S(2)}) async-start(), calls=%async_computation.6 | async-start | bytes 6553600 | tf_op jit(solution)/shard_map/all_gather | solution.py:147
  164.4 9.2 %copy-start.5 = (bf16[512,512]{1,0:T(8,128)(2,1)}, bf16[512,512]{1,0:T(8,128)(2,1)S(1)}, u32[]{:S(2)}) copy-start(bf16[512,512]{1,0:T(8,128)(2,1)S(1)} %get-tuple-element.336) | copy-start | bytes 1572868
  173.6 4.8 %copy-start.2 = (bf16[512,512]{1,0:T(8,128)(2,1)}, bf16[512,512]{1,0:T(8,128)(2,1)S(1)}, u32[]{:S(2)}) copy-start(bf16[512,512]{1,0:T(8,128)(2,1)S(1)} %fusion.52) | copy-start | bytes 1572868
  216.4 95.6 %all-gather.17.cloned.1.call-start = ((), (), s32[]{:S(2)}) async-start(), calls=%async_computation.7 | async-start | bytes 1638400 | tf_op jit(solution)/shard_map/all_gather | solution.py:158
  275.7 4.8 %copy-start.1 = (bf16[8,4,40,2048]{3,2,0,1:T(8,128)(2,1)S(1)}, bf16[8,4,40,2048]{3,2,0,1:T(8,128)(2,1)}, u32[]{:S(2)}) copy-start(bf16[8,4,40,2048]{3,2,0,1:T(8,128)(2,1)} %all-gather.15.cloned.1.call-done) | copy-start | bytes 15728644
  275.7 5.3 %copy-start.13 = (bf16[4,2048,128]{2,1,0:T(8,128)(2,1)S(1)}, bf16[4,2048,128]{2,1,0:T(8,128)(2,1)}, u32[]{:S(2)}) copy-start(bf16[4,2048,128]{2,1,0:T(8,128)(2,1)} %param.29) | copy-start | bytes 6291460
  283.3 65.4 %all-gather.13.cloned.1.call-start = ((), (), s32[]{:S(2)}) async-start(), calls=%async_computation.5 | async-start | bytes 2621440 | tf_op jit(solution)/shard_map/all_gather | solution.py:121
  314.1 5.8 %copy-start.12 = (f32[512,2]{0,1:T(2,128)S(1)}, f32[512,2]{0,1:T(2,128)}, u32[]{:S(2)}) copy-start(f32[512,2]{0,1:T(2,128)} %param.27) | copy-start | bytes 12292
  315.3 47.3 %all-to-all-start.1 = ((bf16[8,4,40,512]{3,2,1,0:T(8,128)(2,1)}), bf16[8,4,40,512]{3,2,1,0:T(8,128)(2,1)S(1)}, u32[]{:S(2)}, u32[]{:S(2)}) async-start(bf16[8,4,40,512]{3,2,1,0:T(8,128)(2,1)} %copy.45), calls=%async_computation.1 | async-start | bytes 2621440 | tf_op jit(solution)/shard_map/all_to_all | solution.py:162
  348.7 2.5 copy-start.3
  348.7 2.5 copy-start.14
  367.7 3.4 copy-start.7
  371.1 4.5 %copy-start.4 = (bf16[512,512]{1,0:T(8,128)(2,1)S(1)}, bf16[512,512]{1,0:T(8,128)(2,1)}, u32[]{:S(2)}) copy-start(bf16[512,512]{1,0:T(8,128)(2,1)} %all_gather.29) | copy-start | bytes 1572868
  371.1 4.5 %copy-start.6 = (bf16[512,512]{1,0:T(8,128)(2,1)S(1)}, bf16[512,512]{1,0:T(8,128)(2,1)}, u32[]{:S(2)}) copy-start(bf16[512,512]{1,0:T(8,128)(2,1)} %copy-done.5) | copy-start | bytes 1572868
  371.1 4.6 %copy-start.8 = (bf16[512,512]{1,0:T(8,128)(2,1)S(1)}, bf16[512,512]{1,0:T(8,128)(2,1)}, u32[]{:S(2)}) copy-start(bf16[512,512]{1,0:T(8,128)(2,1)} %param.33) | copy-start | bytes 1572868
Sparse Core Ops, SparseCore 0:
  8.9 32.0 all-gather.8
  42.6 28.6 all-gather.6
  92.1 69.7 all-gather.10
  216.5 59.1 all-gather.14
  283.4 28.5 all-gather.16
  313.6 35.0 all-gather.12
where the time goes:
time: 385 us; the launch traced here: 384 us
  waiting for transfers between devices  211 us (55%)
  blocking collectives  72.3 us (19%)
  local copies, waits for them, and re-layouts  38.3 us (10%)
  matrix products  20.8 us (5%)
  other arithmetic  17.1 us (4%)
  between operations  13.8 us (4%)
  loops' own time  5.65 us (1%)
  starting transfers between devices  4.99 us (1%)
    all_gather x1, waiting for transfers between devices, shards(): lax.all_gather(lax.all_to_all(outgoing, 'sp', split_axis=0, concat_axis=0...  59 us
    all_gather x1, waiting for transfers between devices, shards(): lax.all_gather(attended, 'tp', axis=1, tiled=True)  54.9 us
    all_to_all x1, blocking collectives, shards(): lax.all_to_all(outgoing, 'sp', split_axis=0, concat_axis=0, tiled=True)  36.8 us
    all_gather x1, waiting for transfers between devices, shards(): hidden_all = lax.all_gather(hidden, 'tp', axis=3, tiled=True)  28.1 us
    all_gather x1, waiting for transfers between devices, shards(): normed = lax.all_gather(normed_own, 'tp', axis=1, tiled=True)  27.9 us
    all_gather x1, waiting for transfers between devices, shards(): key_part = lax.all_gather(key_heads, 'sp', axis=0, tiled=True)  27 us
    all_gather x1, blocking collectives, shards(): all_gates = lax.all_gather(log_gate_sums, 'sp', axis=0, tiled=True)  15.9 us
    all_gather x1, waiting for transfers between devices, shards(): value_part = lax.all_gather(value_heads, 'sp', axis=0, tiled=True)  13.3 us
  transfers between devices with their start and end apart: 7, of which 6 were waited for; matrix products, arithmetic and copies ran while one was open for 7% of the time, Pallas kernels for 0%

commit v1 on v0

--- a/solution.py
+++ b/solution.py
@@ -105,7 +105,7 @@
     attended = attended.transpose(1, 0, 2).reshape(tok_dev, local_heads * head_dim)
     weight_rows = out_weight
     projected = jnp.dot(
-        lax.all_gather(attended, "tp", axis=1, tiled=True),
+        jnp.concatenate(lax.all_gather(attended, "tp"), axis=1),
         weight_rows,
         preferred_element_type=jnp.float32,
     )

time: 385 us -> 387 us (level)
  no operation moved by 1% of the time
where the time goes in v1:
time: 387 us; the launch traced here: 386 us
  waiting for transfers between devices  211 us (55%)
  blocking collectives  72.3 us (19%)
  local copies, waits for them, and re-layouts  41.4 us (11%)
  matrix products  20.8 us (5%)
  other arithmetic  16.4 us (4%)
  between operations  13.8 us (4%)
  loops' own time  5.65 us (1%)
  starting transfers between devices  4.99 us (1%)
    all_gather x1, waiting for transfers between devices, shards(): lax.all_gather(lax.all_to_all(outgoing, 'sp', split_axis=0, concat_axis=0...  59 us
    all_gather x1, waiting for transfers between devices, shards(): lax.all_gather(attended, 'tp')  54.8 us
    all_to_all x1, blocking collectives, shards(): lax.all_to_all(outgoing, 'sp', split_axis=0, concat_axis=0, tiled=True)  36.8 us
    all_gather x1, waiting for transfers between devices, shards(): hidden_all = lax.all_gather(hidden, 'tp', axis=3, tiled=True)  28.1 us
    all_gather x1, waiting for transfers between devices, shards(): normed = lax.all_gather(normed_own, 'tp', axis=1, tiled=True)  27.9 us
    all_gather x1, waiting for transfers between devices, shards(): key_part = lax.all_gather(key_heads, 'sp', axis=0, tiled=True)  27 us
    all_gather x1, blocking collectives, shards(): all_gates = lax.all_gather(log_gate_sums, 'sp', axis=0, tiled=True)  15.9 us
    all_gather x1, waiting for transfers between devices, shards(): value_part = lax.all_gather(value_heads, 'sp', axis=0, tiled=True)  13.3 us
  transfers between devices with their start and end apart: 7, of which 6 were waited for; matrix products, arithmetic and copies ran while one was open for 7% of the time, Pallas kernels for 0%

profile of v1, /device:TPU:0, one launch (start us, length us, event | category | flops | bytes accessed | tf_op | source)
XLA Modules:
  0.0 386.1 jit_solution(5567132486718074868)
XLA Ops:
  11.8 15.9 %all_gather.25 = f32[4096,4]{0,1:T(4,128)S(1)} all-gather(f32[512,4]{0,1:T(4,128)S(1)} %copy-done.9), channel_id=1, replica_groups=mesh['sp'=8,'tp'=4] {'sp'}, dimensions={0}, use_global_device_ids=true | all-gather | bytes 73728 | tf_op jit(solution)/shard_map/all_gather | solution.py:55
  27.7 13.3 %all-gather.9.cloned.1.call-done = bf16[4096,4,64]{0,2,1:T(8,128)(2,1)} async-done(((bf16[512,4,64]{0,2,1:T(8,128)(2,1)}), bf16[4096,4,64]{0,2,1:T(8,128)(2,1)}) %all-gather.9.cloned.1.call-update) | async-done | bytes 2097168 | tf_op jit(solution)/shard_map/all_gather | solution.py:64
  41.0 3.2 copy.74
  44.2 27.0 %all-gather.7.cloned.1.call-done = bf16[4096,4,64]{0,2,1:T(8,128)(2,1)} async-done(((bf16[512,4,64]{0,2,1:T(8,128)(2,1)}), bf16[4096,4,64]{0,2,1:T(8,128)(2,1)}) %all-gather.7.cloned.1.call-update) | async-done | bytes 2097168 | tf_op jit(solution)/shard_map/all_gather | solution.py:63
  71.3 3.2 copy.75
  74.6 16.6 %while.17 = (s32[]{:T(128)}, f32[4,512]{1,0:T(4,128)S(1)}, f32[4,512]{1,0:T(4,128)S(1)}, f32[4,512,64]{1,2,0:T(8,128)S(1)}, s32[8]{0:T(128)S(1)}, /*index=5*/s32...) while((s32[]{:T(128)}, f32[4,512]{1,0:T(4,128)S(1)}, ...), condition=%wide.region_5.6_spmd.clone, body=%wide.region_0.5_spmd.clone.sunk | while | flops 286790656 | bytes 15676785 | solution.py:102
  75.8 6.3 %conditional.3 = ((f32[4,512]{1,0:T(4,128)S(1)}, f32[4,512]{1,0:T(4,128)S(1)}, f32[4,512,64]{1,2,0:T(8,128)S(1)})) conditional(s32[]{:T(128)} %convert_element_type.105, (f32[4,512]{1,0:T(4,128)S(1)}, f32[4,512]{1,0:T(4,128)S(1)}, f32[4,512,64]{1,2,0:T(8,128)S(1)}) %tuple.51, (s32[]{:T(128)}, s32[]{:T(128)}, bf16[8,512,4,64]{1,3,2,0:T(8,128)(2,1)}, ...), branch_computations={%region_1.1_spmd, %region_2.4_spmd} | conditional | flops 286790656 | bytes 15674446 | solution.py:99
  92.2 9.0 %reduce-window.6 = s32[32,8,128]{2,1,0:T(8,128)S(1)} reduce-window(s32[32,8,128]{2,1,0:T(8,128)S(1)} %fusion.56, s32[]{:T(128)} %constant.93.clone.1), window={size=1x1x128 pad=0_0x0_0x127_0}, to_apply=%region_8.9 | reduce-window | flops 4161536 | bytes 262148 | tf_op jit(solution)/shard_map/reduce-window
  102.1 4.3 %scatter_custom_fusion = s32[1280]{0:T(1024)S(1)} fusion(s32[1024]{0:T(1024)S(1)} %bitcast.133, s32[1024]{0:T(1024)S(1)} %add_select_fusion, s32[]{:T(128)} %constant.98.clone.1), kind=kCustom, calls=%fused_computation.75 | custom fusion | bytes 5124 | tf_op jit(solution)/shard_map/scatter | solution.py:141
  107.2 54.8 %all-gather.11.cloned.1.call-done = bf16[4,512,256]{2,1,0:T(8,128)(2,1)} async-done(((bf16[1,512,256]{2,1,0:T(8,128)(2,1)}), bf16[4,512,256]{2,1,0:T(8,128)(2,1)}) %all-gather.11.cloned.1.call-update) | async-done | bytes 1048592 | tf_op jit(solution)/shard_map/all_gather | solution.py:108
  164.3 2.5 fusion.50
  166.8 8.9 %psum.7 = f32[512]{0:T(512)S(1)} all-reduce(f32[512]{0:T(512)S(1)} %get-tuple-element.347), channel_id=1, replica_groups=mesh['sp'=8,'tp'=4] {'tp'}, use_global_device_ids=true, to_apply=%region_7.8 | all-reduce | flops 512 | bytes 4096 | tf_op jit(solution)/shard_map/psum | solution.py:115
  176.0 4.7 %gather_fusion = bf16[1280,512]{1,0:T(8,128)(2,1)} fusion(bf16[513,512]{1,0:T(8,128)(2,1)S(1)} %concatenate.3, s32[2048]{0:T(1024)S(1)} %pad_clamp_fusion), kind=kCustom, calls=%fused_computation | custom fusion | bytes 2626560 | tf_op jit(solution)/shard_map/gather | solution.py:146
  180.8 36.8 %all_to_all.10 = bf16[8,4,40,512]{3,2,1,0:T(8,128)(2,1)S(1)} all-to-all(bf16[8,4,40,512]{3,2,1,0:T(8,128)(2,1)} %bitcast.119), channel_id=1, replica_groups=mesh['sp'=8,'tp'=4] {'sp'}, dimensions={0} | all-to-all | bytes 2621440 | tf_op jit(solution)/shard_map/all_to_all | solution.py:148
  219.0 59.0 %all-gather.15.cloned.1.call-done = bf16[8,4,40,2048]{3,2,0,1:T(8,128)(2,1)} async-done(((bf16[8,4,40,512]{3,2,0,1:T(8,128)(2,1)}), bf16[8,4,40,2048]{3,2,0,1:T(8,128)(2,1)}) %all-gather.15.cloned.1.call-update) | async-done | bytes 5242896 | tf_op jit(solution)/shard_map/all_gather | solution.py:147
  278.1 4.8 %fusion.37 = f32[8,4,40,128]{3,2,0,1:T(8,128)S(1)} fusion(bf16[8,4,40,2048]{3,2,0,1:T(8,128)(2,1)} %all-gather.15.cloned.1.call-done, bf16[4,2048,128]{2,1,0:T(8,128)(2,1)} %param.28), kind=kOutput, calls=%fused_computation.48 | convolution fusion | flops 671088640 | bytes 7995392 | tf_op jit(solution)/shard_map/secd,edf->secf/dot_general | solution.py:153
  286.2 28.1 %all-gather.17.cloned.1.call-done = bf16[8,4,40,512]{3,2,0,1:T(8,128)(2,1)} async-done(((bf16[8,4,40,128]{3,2,0,1:T(8,128)(2,1)}), bf16[8,4,40,512]{3,2,0,1:T(8,128)(2,1)}) %all-gather.17.cloned.1.call-update) | async-done | bytes 1310736 | tf_op jit(solution)/shard_map/all_gather | solution.py:158
  317.7 4.6 %all-to-all-start.1 = ((bf16[8,4,40,512]{3,2,1,0:T(8,128)(2,1)}), bf16[8,4,40,512]{3,2,1,0:T(8,128)(2,1)S(1)}, u32[]{:S(2)}, u32[]{:S(2)}) async-start(bf16[8,4,40,512]{3,2,1,0:T(8,128)(2,1)} %copy.62), calls=%async_computation.1 | async-start | bytes 2621440 | tf_op jit(solution)/shard_map/all_to_all | solution.py:162
  323.2 27.9 %all-gather.13.cloned.1.call-done = bf16[512,2048]{1,0:T(8,128)(2,1)} async-done(((bf16[512,512]{1,0:T(8,128)(2,1)}), bf16[512,2048]{1,0:T(8,128)(2,1)}) %all-gather.13.cloned.1.call-update) | async-done | bytes 2097168 | tf_op jit(solution)/shard_map/all_gather | solution.py:121
  351.1 2.5 fusion.62
  354.4 10.6 %all_gather.29 = bf16[512,512]{1,0:T(8,128)(2,1)} all-gather(bf16[512,128]{1,0:T(8,128)(2,1)S(1)} %fusion.49), channel_id=1, replica_groups=mesh['sp'=8,'tp'=4] {'tp'}, dimensions={1}, use_global_device_ids=true | all-gather | bytes 655360 | tf_op jit(solution)/shard_map/all_gather | solution.py:128
  365.0 5.1 %gather_fusion.1 = bf16[1024,512]{1,0:T(8,128)(2,1)} fusion(bf16[1280,512]{1,0:T(8,128)(2,1)S(1)} %bitcast.118, s32[1024]{0:T(1024)S(1)} %broadcast_clamp_fusion), kind=kCustom, calls=%fused_computation.1 | custom fusion | bytes 2101248 | tf_op jit(solution)/shard_map/gather | solution.py:164
  370.1 3.4 reshape.128
  373.5 4.5 %multiply_reduce_fusion = f32[512,512]{1,0:T(8,128)S(1)} fusion(f32[512,2,512]{2,1,0:T(2,128)} %reshape.128, f32[512,2]{1,0:T(8,128)S(1)} %copy-done.7), kind=kLoop, calls=%fused_computation.38 | loop fusion | flops 786432 | bytes 3149824 | tf_op jit(solution)/shard_map/reduce_sum | solution.py:165
  (115 shorter events, 32.3 us)
Async XLA Ops:
  6.5 307.8 %copy-start = (bf16[4,512,512]{2,1,0:T(8,128)(2,1)S(1)}, bf16[4,512,512]{2,1,0:T(8,128)(2,1)}, u32[]{:S(2)}) copy-start(bf16[4,512,512]{2,1,0:T(8,128)(2,1)} %param.30) | copy-start | bytes 6291460
  6.5 5.1 %copy-start.10 = (bf16[512,256]{1,0:T(8,128)(2,1)S(1)}, bf16[512,256]{1,0:T(8,128)(2,1)}, u32[]{:S(2)}) copy-start(bf16[512,256]{1,0:T(8,128)(2,1)} %param.19) | copy-start | bytes 786436
  6.5 5.2 %copy-start.9 = (f32[512,4]{0,1:T(4,128)S(1)}, f32[512,4]{0,1:T(4,128)}, u32[]{:S(2)}) copy-start(f32[512,4]{0,1:T(4,128)} %param.22) | copy-start | bytes 24580
  6.5 34.5 %all-gather.9.cloned.1.call-start = ((), (), s32[]{:S(2)}) async-start(), calls=%async_computation.3 | async-start | bytes 2359296 | tf_op jit(solution)/shard_map/all_gather | solution.py:64
  8.5 62.8 %all-gather.7.cloned.1.call-start = ((), (), s32[]{:S(2)}) async-start(), calls=%async_computation.2 | async-start | bytes 2359296 | tf_op jit(solution)/shard_map/all_gather | solution.py:63
  10.4 151.6 %all-gather.11.cloned.1.call-start = ((), (), s32[]{:S(2)}) async-start(), calls=%async_computation.4 | async-start | bytes 1310720 | tf_op jit(solution)/shard_map/all_gather | solution.py:108
  91.2 10.4 %copy-start.11 = (s32[512,2]{0,1:T(2,128)S(1)}, s32[512,2]{0,1:T(2,128)}, u32[]{:S(2)}) copy-start(s32[512,2]{0,1:T(2,128)} %param.26) | copy-start | bytes 12292
  92.1 186.0 %all-gather.15.cloned.1.call-start = ((), (), s32[]{:S(2)}) async-start(), calls=%async_computation.6 | async-start | bytes 6553600 | tf_op jit(solution)/shard_map/all_gather | solution.py:147
  166.8 9.2 %copy-start.5 = (bf16[512,512]{1,0:T(8,128)(2,1)}, bf16[512,512]{1,0:T(8,128)(2,1)S(1)}, u32[]{:S(2)}) copy-start(bf16[512,512]{1,0:T(8,128)(2,1)S(1)} %get-tuple-element.348) | copy-start | bytes 1572868
  176.0 4.8 %copy-start.2 = (bf16[512,512]{1,0:T(8,128)(2,1)}, bf16[512,512]{1,0:T(8,128)(2,1)S(1)}, u32[]{:S(2)}) copy-start(bf16[512,512]{1,0:T(8,128)(2,1)S(1)} %fusion.52) | copy-start | bytes 1572868
  218.8 95.6 %all-gather.17.cloned.1.call-start = ((), (), s32[]{:S(2)}) async-start(), calls=%async_computation.7 | async-start | bytes 1638400 | tf_op jit(solution)/shard_map/all_gather | solution.py:158
  278.1 4.8 %copy-start.1 = (bf16[8,4,40,2048]{3,2,0,1:T(8,128)(2,1)S(1)}, bf16[8,4,40,2048]{3,2,0,1:T(8,128)(2,1)}, u32[]{:S(2)}) copy-start(bf16[8,4,40,2048]{3,2,0,1:T(8,128)(2,1)} %all-gather.15.cloned.1.call-done) | copy-start | bytes 15728644
  278.1 5.3 %copy-start.13 = (bf16[4,2048,128]{2,1,0:T(8,128)(2,1)S(1)}, bf16[4,2048,128]{2,1,0:T(8,128)(2,1)}, u32[]{:S(2)}) copy-start(bf16[4,2048,128]{2,1,0:T(8,128)(2,1)} %param.29) | copy-start | bytes 6291460
  285.7 65.4 %all-gather.13.cloned.1.call-start = ((), (), s32[]{:S(2)}) async-start(), calls=%async_computation.5 | async-start | bytes 2621440 | tf_op jit(solution)/shard_map/all_gather | solution.py:121
  316.5 5.8 %copy-start.12 = (f32[512,2]{0,1:T(2,128)S(1)}, f32[512,2]{0,1:T(2,128)}, u32[]{:S(2)}) copy-start(f32[512,2]{0,1:T(2,128)} %param.27) | copy-start | bytes 12292
  317.7 47.3 %all-to-all-start.1 = ((bf16[8,4,40,512]{3,2,1,0:T(8,128)(2,1)}), bf16[8,4,40,512]{3,2,1,0:T(8,128)(2,1)S(1)}, u32[]{:S(2)}, u32[]{:S(2)}) async-start(bf16[8,4,40,512]{3,2,1,0:T(8,128)(2,1)} %copy.62), calls=%async_computation.1 | async-start | bytes 2621440 | tf_op jit(solution)/shard_map/all_to_all | solution.py:162
  351.1 2.5 copy-start.3
  351.1 2.5 copy-start.14
  370.1 3.4 copy-start.7
  373.5 4.5 %copy-start.4 = (bf16[512,512]{1,0:T(8,128)(2,1)S(1)}, bf16[512,512]{1,0:T(8,128)(2,1)}, u32[]{:S(2)}) copy-start(bf16[512,512]{1,0:T(8,128)(2,1)} %all_gather.29) | copy-start | bytes 1572868
  373.5 4.5 %copy-start.6 = (bf16[512,512]{1,0:T(8,128)(2,1)S(1)}, bf16[512,512]{1,0:T(8,128)(2,1)}, u32[]{:S(2)}) copy-start(bf16[512,512]{1,0:T(8,128)(2,1)} %copy-done.5) | copy-start | bytes 1572868
  373.5 4.6 %copy-start.8 = (bf16[512,512]{1,0:T(8,128)(2,1)S(1)}, bf16[512,512]{1,0:T(8,128)(2,1)}, u32[]{:S(2)}) copy-start(bf16[512,512]{1,0:T(8,128)(2,1)} %param.33) | copy-start | bytes 1572868
Sparse Core Ops, SparseCore 0:
  8.9 32.0 all-gather.8
  42.6 28.6 all-gather.6
  92.2 69.7 all-gather.10
  218.9 59.1 all-gather.14
  285.8 28.5 all-gather.16
  316.0 35.0 all-gather.12
